TPU v7x, 32 devices: a whole 2x2x4 slice. The times are simulated.
32 devices in a mesh: ep: 8 (over z, y), tp: 4 (over x, core).
Axes of the slice: x: 2, y: 2, z: 4, core: 2. Of those that a mesh axis runs over, the one named last changes fastest.
Arguments:
- q_heads: bfloat16 [8192, 1024], P('ep', 'tp'), may hold values from -200 to 200
- k_heads: bfloat16 [8192, 256], P('ep', 'tp'), may hold values from -6 to 6
- v_heads: bfloat16 [8192, 256], P('ep', 'tp'), may hold values from -6 to 6
- sink_logits: float32 [16], P('tp'), may hold values from 1 to 5
- out_weight: bfloat16 [1024, 2048], P(None, 'tp'), may hold values from -1.5 to 1.5
- tokens_b: bfloat16 [4096, 2048], P('ep'), may hold values from -6 to 6
- moe_gain: float32 [2048], replicated, may hold values from 0.1 to 1.9
- router_group: bfloat16 [2048, 4], replicated, may hold values from -0.125 to 0.125
- router_expert: bfloat16 [2048, 16], replicated, may hold values from -0.125 to 0.125
- route_expert: int32 [4096, 2], P('ep'), may hold values from 0 to 15, as said below
- expert_gate: bfloat16 [16, 2048, 1024], P('ep', None, 'tp'), may hold values from -0.125 to 0.125
- expert_up: bfloat16 [16, 2048, 1024], P('ep', None, 'tp'), may hold values from -0.125 to 0.125
- expert_down: bfloat16 [16, 1024, 2048], P('ep', 'tp'), may hold values from -0.75 to 0.75
Outputs:
- mixer_out: bfloat16 [8192, 2048], P('ep', 'tp')
- moe_out: bfloat16 [4096, 2048], P(('ep', 'tp'))
Inputs may be any that keep to these rules, and one draw needn't show every extreme that they name: `route_expert`: each token names two different experts, in rising order, of one group of 4 consecutive experts. In each aligned block of 128 rows (the rows of one device) no expert is named by more than 32 tokens, in each group one expert is named by exactly 32 tokens of every block, and each group is named by a quarter of every block's tokens.
All inputs are finite; a program needn't handle non-finite values.
Results may differ from a plain program's by a relative error of at most 0.011.
Values may be sent and summed in bfloat16 or wider, within the bound.
No kernel may reach another device: no remote copies, remote signals or barrier semaphores. Data moves between devices by JAX's collectives and lax.ppermute only.
A program may use at most 128 MiB of HBM per device.

v0:
```python
import jax
import jax.numpy as jnp
from jax import lax
from jax.sharding import PartitionSpec as P

HEADS = 16
KV = 4
HD = 64
WINDOW = 128


def shifted(value, axis, steps):
    count = lax.axis_size(axis)
    leading, last = (max(0, -steps), min(count, count - steps))
    return lax.ppermute(value, axis, [(source, source + steps) for source in range(leading, last)])


def normalize(rows_in, gain):
    values = rows_in.astype(jnp.float32)
    scaled = values * lax.rsqrt(jnp.mean(values * values, axis=-1, keepdims=True) + 1e-06) * gain
    return scaled.astype(jnp.bfloat16)


def gate_weights(normed, routes, router_group, router_expert):
    group_logits = jnp.dot(normed, router_group, preferred_element_type=jnp.float32)
    expert_logits = jnp.dot(normed, router_expert, preferred_element_type=jnp.float32)
    group_count = router_group.shape[1]
    expert_count = router_expert.shape[1]
    chosen_group = routes[:, 0] // (expert_count // group_count)
    group_match = chosen_group[:, None] == jnp.arange(group_count, dtype=jnp.int32)[None, :]
    group_share = jnp.sum(
        jnp.where(group_match, jax.nn.softmax(group_logits, axis=-1), 0.0), axis=-1
    )
    expert_match = routes[:, :, None] == jnp.arange(expert_count, dtype=jnp.int32)[None, None, :]
    picked = jnp.sum(jnp.where(expert_match, expert_logits[:, None, :], 0.0), axis=-1)
    return group_share[:, None] * jax.nn.softmax(picked, axis=-1)


def slot_positions(routes, sub_count, expert_count):
    flat_routes = routes.reshape(sub_count, -1)
    onehot = (
        flat_routes[:, :, None] == jnp.arange(expert_count, dtype=jnp.int32)[None, None, :]
    ).astype(jnp.int32)
    places = jnp.sum(onehot * jnp.cumsum(onehot, axis=1), axis=2) - 1
    return (flat_routes, places)


def fill_slots(normed, flat_routes, places, sub_count, expert_count, capacity, exp_local):
    sub_index = jnp.arange(sub_count, dtype=jnp.int32)[:, None]
    target = ((flat_routes * sub_count + sub_index) * capacity + places).reshape(-1)
    source = jnp.repeat(normed, 2, axis=0)
    buffer = jnp.zeros((expert_count * sub_count * capacity, normed.shape[1]), jnp.bfloat16)
    buffer = buffer.at[target].set(source)
    return buffer.reshape(
        expert_count // exp_local, exp_local, sub_count, capacity, normed.shape[1]
    )


def per_device(
    q_heads,
    k_heads,
    v_heads,
    sink_logits,
    out_weight,
    tokens_b,
    moe_gain,
    router_group,
    router_expert,
    route_expert,
    expert_gate,
    expert_up,
    expert_down,
):
    span_len = WINDOW
    row_count = q_heads.shape[0]
    kv_local = k_heads.shape[1] // HD
    group_size = HEADS // KV
    blocks = row_count // span_len
    stacked = jnp.stack([k_heads[row_count - span_len :], v_heads[row_count - span_len :]])
    earlier = shifted(stacked, "ep", 1)

    def make_band(own_rows, prev_rows):
        extended = jnp.concatenate([prev_rows, own_rows], axis=0).reshape(
            blocks + 1, span_len, kv_local, HD
        )
        return jnp.concatenate([extended[:-1], extended[1:]], axis=1)

    key_band = make_band(k_heads, earlier[0])
    value_band = make_band(v_heads, earlier[1])
    query_blocks = q_heads.reshape(blocks, span_len, kv_local, group_size, HD)
    scores = jnp.einsum(
        "nqhgd,nkhd->nhgqk", query_blocks, key_band, preferred_element_type=jnp.float32
    ) * HD ** (-0.5)
    first_row = lax.axis_index("ep") * row_count
    query_index = jnp.arange(span_len, dtype=jnp.int32)[:, None]
    key_index = jnp.arange(2 * span_len, dtype=jnp.int32)[None, :]
    distance = query_index + span_len - key_index
    key_place = (
        first_row
        + jnp.arange(blocks, dtype=jnp.int32)[:, None, None] * span_len
        + key_index[None]
        - span_len
    )
    allowed = (distance >= 0)[None] & (distance < span_len)[None] & (key_place >= 0)
    masked = jnp.where(allowed[:, None, None], scores, -1e30)
    sink_full = sink_logits.reshape(kv_local, group_size)[None, :, :, None]
    row_max = jnp.maximum(jnp.max(masked, axis=-1), sink_full)
    weights_exp = jnp.exp(masked - row_max[..., None])
    denominator = jnp.sum(weights_exp, axis=-1) + jnp.exp(sink_full - row_max)
    probs = (weights_exp / denominator[..., None]).astype(jnp.bfloat16)
    attended = jnp.einsum(
        "nhgqk,nkhd->nqhgd", probs, value_band, preferred_element_type=jnp.float32
    )
    attended = attended.astype(jnp.bfloat16).reshape(row_count, kv_local * group_size * HD)
    mixed = jnp.dot(
        lax.all_gather(attended, "tp", axis=1, tiled=True),
        out_weight,
        preferred_element_type=jnp.float32,
    )
    mixer_out = mixed.astype(jnp.bfloat16)
    tp_count = lax.axis_size("tp")
    tp_index = lax.axis_index("tp")
    exp_local = expert_gate.shape[0]
    expert_count = exp_local * lax.axis_size("ep")
    rows_dev = tokens_b.shape[0] // tp_count
    capacity = min(4 * rows_dev // expert_count, rows_dev // 4)
    own_routes = lax.dynamic_slice_in_dim(route_expert, tp_index * rows_dev, rows_dev, 0)
    own_normed = normalize(
        lax.dynamic_slice_in_dim(tokens_b, tp_index * rows_dev, rows_dev, 0), moe_gain
    )
    flat_routes, places = slot_positions(own_routes, 1, expert_count)
    buffer = fill_slots(own_normed, flat_routes, places, 1, expert_count, capacity, exp_local)
    delivered = lax.all_to_all(buffer, "ep", split_axis=0, concat_axis=0, tiled=True)
    arrived = lax.all_gather(delivered, "tp", axis=2, tiled=True)
    own_flat = flat_routes[0]
    own_places = places[0]
    gates = gate_weights(own_normed, own_routes, router_group, router_expert)
    gate_pre = jnp.einsum(
        "setcd,edf->setcf", arrived, expert_gate, preferred_element_type=jnp.float32
    )
    up_pre = jnp.einsum("setcd,edf->setcf", arrived, expert_up, preferred_element_type=jnp.float32)
    activated = (jax.nn.silu(gate_pre) * up_pre).astype(jnp.bfloat16)
    partial_value = jnp.einsum(
        "setcf,efd->setcd", activated, expert_down, preferred_element_type=jnp.float32
    )
    summed = lax.psum_scatter(
        partial_value.astype(jnp.bfloat16), "tp", scatter_dimension=2, tiled=True
    )
    returned = lax.all_to_all(summed, "ep", split_axis=0, concat_axis=0, tiled=True)
    returned = returned.reshape(expert_count * capacity, returned.shape[-1])
    picked_rows = returned[own_flat * capacity + own_places].reshape(
        rows_dev, 2, returned.shape[-1]
    )
    moe_out = jnp.sum(gates[:, :, None] * picked_rows.astype(jnp.float32), axis=1).astype(
        jnp.bfloat16
    )
    return (mixer_out, moe_out)


def solution(mesh):
    in_specs = (
        P("ep", "tp"),
        P("ep", "tp"),
        P("ep", "tp"),
        P("tp"),
        P(None, "tp"),
        P("ep", None),
        P(),
        P(),
        P(),
        P("ep", None),
        P("ep", None, "tp"),
        P("ep", None, "tp"),
        P("ep", "tp", None),
    )
    out_specs = (P("ep", "tp"), P(("ep", "tp"), None))
    return jax.shard_map(
        per_device, mesh=mesh, in_specs=in_specs, out_specs=out_specs, check_vma=False
    )
```

profile of v0, /device:TPU:0, one launch (start us, length us, event | category | flops | bytes accessed | tf_op | source)
XLA Modules:
  0.0 384.7 jit_solution(17518008943013169215)
XLA Ops:
  7.2 0.0 copy-start
  7.2 0.0 all-gather.5.cloned.1.call-start
  7.2 0.8 broadcast_multiply_fusion
  8.1 0.1 copy.64
  8.2 0.1 eq.62
  8.3 0.6 reduce-window.6
  8.9 0.2 slice_reduce_fusion
  9.2 0.1 copy.67
  9.3 0.1 broadcast.263
  9.3 0.1 fusion.41
  9.4 0.1 copy.63
  9.5 0.1 mul.115
  9.7 1.2 fusion.24
  10.9 1.3 fusion.26
  12.2 1.6 broadcast_in_dim.34
  13.8 2.3 reshape.383
  16.0 4.4 %scatter_custom_fusion = bf16[512,2048]{1,0:T(8,128)(2,1)} fusion(s32[256]{0:T(256)S(1)} %bitcast.171, bf16[256,2048]{1,0:T(8,128)(2,1)} %reshape.383, bf16[]{:T(256)} %constant.67.clone.1), kind=kCustom, calls=%fused_computation.35 | custom fusion | bytes 2097664 | tf_op jit(solution)/shard_map/scatter | solution.py:53
  20.5 55.5 %all_to_all.10 = bf16[8,2,1,32,2048]{4,3,2,1,0:T(8,128)(2,1)S(1)} all-to-all(bf16[8,2,1,32,2048]{4,3,2,1,0:T(8,128)(2,1)} %bitcast.159), channel_id=1, replica_groups=mesh['ep'=8,'tp'=4] {'ep'}, dimensions={0} | all-to-all | bytes 4194304 | tf_op jit(solution)/shard_map/all_to_all | solution.py:133
  76.0 1.5 copy.69
  77.5 0.0 all-gather.5.cloned.1.call-update
  77.5 0.0 all-reduce.3.cloned.1.call-start
  77.6 57.4 %all-gather.5.cloned.1.call-done = bf16[8,2,4,32,2048]{4,3,2,0,1:T(8,128)(2,1)} async-done(((bf16[8,2,1,32,2048]{4,3,2,0,1:T(8,128)(2,1)}), bf16[8,2,4,32,2048]{4,3,2,0,1:T(8,128)(2,1)}) %all-gather.5.cloned.1.call-update) | async-done | bytes 8388624 | tf_op jit(solution)/shard_map/all_gather | solution.py:134
  134.9 7.7 %fusion.3 = f32[2,8,4,32,256]{4,3,2,1,0:T(8,128)} fusion(bf16[8,2,4,32,2048]{4,3,2,0,1:T(8,128)(2,1)} %all-gather.5.cloned.1.call-done, bf16[2,2048,256]{2,1,0:T(8,128)(2,1)} %param.24), kind=kOutput, calls=%fused_computation.9 | convolution fusion | flops 2147483648 | bytes 12582912 | tf_op jit(solution)/shard_map/setcd,edf->setcf/dot_general | solution.py:141
  142.6 0.0 copy-done
  142.6 13.5 %convert_bitcast_fusion = bf16[8,2,4,32,2048]{4,3,2,0,1:T(8,128)(2,1)} fusion(bf16[2,256,2048]{2,1,0:T(8,128)(2,1)S(1)} %copy-done, f32[2,8,4,32,256]{4,3,2,1,0:T(8,128)} %fusion.3, bf16[8,2,4,32,2048]{4,3,2,0,1:T(8,128)(2,1)} %all-gather.5.cloned.1.call-done, bf16[2,2048,256]{2,1,0:T(8,128)(2,1)} %param.23), kind=kOutput, calls=%fused_computation.2 | convolution fusion | flops 4302307328 | bytes 23068672 | tf_op jit(solution)/shard_map/setcf,efd->setcd/dot_general | solution.py:143
  156.1 0.0 all-reduce.3.cloned.1.call-update
  156.1 0.9 copy-done.3
  157.0 0.1 copy-done.4
  157.1 3.6 collective-permute-start
  160.7 0.1 add_compare_fusion
  160.8 0.3 broadcast_and_fusion
  161.2 0.0 copy-done.5
  161.2 0.4 reshape.392
  161.7 0.0 copy-done.9
  161.7 0.6 dynamic-slice
  162.3 0.0 collective-permute-done
  162.5 0.0 copy-start.8
  162.5 0.9 fusion.1
  163.4 0.0 copy-start.2
  163.4 0.0 copy-done.8
  163.4 0.1 broadcast_maximum_fusion
  163.5 1.1 fusion
  164.5 0.8 copy-done.2
  165.3 0.1 exponential_add_fusion
  165.4 143.8 %all-reduce.3.cloned.1.call-done = bf16[8,2,4,32,2048]{4,3,2,0,1:T(8,128)(2,1)} async-done(((bf16[8,2,4,32,2048]{4,3,2,0,1:T(8,128)(2,1)}), bf16[8,2,4,32,2048]{4,3,2,0,1:T(8,128)(2,1)}) %all-reduce.3.cloned.1.call-update) | async-done | bytes 8388624
  309.2 2.5 constant_dynamic-slice_fusion
  311.6 1.6 copy.70
  313.2 5.5 %all-to-all-start.1 = ((bf16[8,2,1,32,2048]{4,3,2,1,0:T(8,128)(2,1)}), bf16[8,2,1,32,2048]{4,3,2,1,0:T(8,128)(2,1)S(1)}, u32[]{:S(2)}, u32[]{:S(2)}) async-start(bf16[8,2,1,32,2048]{4,3,2,1,0:T(8,128)(2,1)} %copy.70), calls=%async_computation.1 | async-start | bytes 4194304 | tf_op jit(solution)/shard_map/all_to_all | solution.py:149
  318.8 0.0 all-gather.3.cloned.1.call-start
  318.8 3.4 fusion.21
  322.2 0.0 copy-start.7
  322.2 0.3 copy.61
  322.6 0.9 copy.91
  323.5 0.0 all-gather.3.cloned.1.call-update
  323.5 0.0 copy-done.6
  323.5 0.2 fusion.52
  323.8 0.3 fusion.51
  324.2 0.1 copy.62
  324.3 22.5 %all-gather.3.cloned.1.call-done = bf16[1024,1024]{0,1:T(8,128)(2,1)} async-done(((bf16[1024,256]{0,1:T(8,128)(2,1)}), bf16[1024,1024]{0,1:T(8,128)(2,1)}) %all-gather.3.cloned.1.call-update) | async-done | bytes 2097168 | tf_op jit(solution)/shard_map/all_gather | solution.py:116
  346.8 4.1 %convolution_convert_fusion = bf16[1024,512]{1,0:T(8,128)(2,1)} fusion(bf16[1024,1024]{0,1:T(8,128)(2,1)} %all-gather.3.cloned.1.call-done, bf16[1024,512]{1,0:T(8,128)(2,1)} %param.17), kind=kOutput, calls=%fused_computation.24 | convolution fusion | flops 1074266112 | bytes 4194304 | tf_op jit(solution)/shard_map/dot_general | solution.py:115
  350.9 15.8 %all-to-all-done.1 = bf16[8,2,1,32,2048]{4,3,2,1,0:T(8,128)(2,1)S(1)} async-done(((bf16[8,2,1,32,2048]{4,3,2,1,0:T(8,128)(2,1)}), bf16[8,2,1,32,2048]{4,3,2,1,0:T(8,128)(2,1)S(1)}, u32[]{:S(2)}, u32[]{:S(2)}) %all-to-all-start.1) | async-done | bytes 2097184 | tf_op jit(solution)/shard_map/all_to_all | solution.py:149
  366.7 2.3 gather_fusion
  369.0 3.5 reshape.370
  372.6 5.6 %multiply_reduce_fusion = bf16[128,2048]{1,0:T(8,128)(2,1)} fusion(f32[128,2,2048]{2,1,0:T(2,128)} %reshape.370, f32[128,2]{1,0:T(8,128)S(1)} %copy.62), kind=kLoop, calls=%fused_computation.22 | loop fusion | flops 786432 | bytes 2622464 | tf_op jit(solution)/shard_map/reduce_sum | solution.py:154
  (40 shorter events, 0.5 us)
Async XLA Ops:
  7.2 135.4 %copy-start = (bf16[2,256,2048]{2,1,0:T(8,128)(2,1)S(1)}, bf16[2,256,2048]{2,1,0:T(8,128)(2,1)}, u32[]{:S(2)}) copy-start(bf16[2,256,2048]{2,1,0:T(8,128)(2,1)} %param.25) | copy-start | bytes 6291460
  7.2 127.8 %all-gather.5.cloned.1.call-start = ((), (), s32[]{:S(2)}) async-start(), calls=%async_computation.3 | async-start | bytes 10485760 | tf_op jit(solution)/shard_map/all_gather | solution.py:134
  77.5 231.6 %all-reduce.3.cloned.1.call-start = ((), (), s32[]{:S(2)}) async-start(), calls=%async_computation.4 | async-start | bytes 16777216
  156.1 0.9 copy-start.3
  156.1 1.0 copy-start.4
  156.1 5.1 %copy-start.5 = (bf16[1024,256]{1,0:T(8,128)(2,1)S(1)}, bf16[1024,256]{1,0:T(8,128)(2,1)}, u32[]{:S(2)}) copy-start(bf16[1024,256]{1,0:T(8,128)(2,1)} %param.13) | copy-start | bytes 1572868
  157.1 4.6 %copy-start.9 = (u32[32]{0:T(128)S(1)}, u32[32]{0:T(128)}, u32[]{:S(2)}) copy-start(u32[32]{0:T(128)} %constant.75) | copy-start | bytes 388
  157.1 5.2 %collective-permute-start = (bf16[2,128,64]{1,2,0:T(8,128)(2,1)S(1)}, bf16[2,128,64]{1,2,0:T(8,128)(2,1)S(1)}, u32[]{:S(2)}, u32[]{:S(2)}) collective-permute-start(bf16[2,128,64]{1,2,0:T(8,128)(2,1)S(1)} %pad_maximum_fusion.2), channel_id=1, source_target_pairs={{0,4},{4,8},{8,12},{12,16},{16,20},{20,24},{24,28},{1,5},{5,9},{9,... | collective-permute-start | bytes 98312 | tf_op jit(solution)/shard_map/ppermute | solution.py:15
  162.5 0.9 copy-start.8
  163.4 1.9 copy-start.2
  313.2 53.4 %all-to-all-start.1 = ((bf16[8,2,1,32,2048]{4,3,2,1,0:T(8,128)(2,1)}), bf16[8,2,1,32,2048]{4,3,2,1,0:T(8,128)(2,1)S(1)}, u32[]{:S(2)}, u32[]{:S(2)}) async-start(bf16[8,2,1,32,2048]{4,3,2,1,0:T(8,128)(2,1)} %copy.70), calls=%async_computation.1 | async-start | bytes 4194304 | tf_op jit(solution)/shard_map/all_to_all | solution.py:149
  318.8 28.0 %all-gather.3.cloned.1.call-start = ((), (), s32[]{:S(2)}) async-start(), calls=%async_computation.2 | async-start | bytes 2621440 | tf_op jit(solution)/shard_map/all_gather | solution.py:116
  322.2 1.3 copy-start.6
  322.2 1.6 copy-start.7
  369.0 9.1 %copy-start.1 = (bf16[2,256,2048]{2,1,0:T(8,128)(2,1)S(1)}, bf16[2,256,2048]{2,1,0:T(8,128)(2,1)}, u32[]{:S(2)}) copy-start(bf16[2,256,2048]{2,1,0:T(8,128)(2,1)} %param.25) | copy-start | bytes 6291460
Sparse Core Ops, SparseCore 0:
  77.6 57.2 all-gather.4
  156.3 152.8 all-reduce.2
  323.6 23.1 all-gather.2
where the time goes:
time: 385 us
  waiting for transfers between devices  239 us (62%)
  blocking collectives  55.5 us (14%)
  matrix products  30.1 us (8%)
  local copies, waits for them, and re-layouts  24.9 us (6%)
  between operations  14.1 us (4%)
  other arithmetic  11.5 us (3%)
  starting transfers between devices  9.2 us (2%)
    unnamed x4, waiting for transfers between devices  144 us
    all_gather x1, waiting for transfers between devices, per_device(): arrived = lax.all_gather(delivered, 'tp', axis=2, tiled=True)  57.4 us
    all_to_all x1, blocking collectives, per_device(): lax.all_to_all(buffer, 'ep', split_axis=0, concat_axis=0, tiled=True)  55.5 us
    all_gather x1, waiting for transfers between devices, per_device(): lax.all_gather(attended, 'tp', axis=1, tiled=True)  22.5 us
    all_to_all x1, waiting for transfers between devices, per_device(): lax.all_to_all(summed, 'ep', split_axis=0, concat_axis=0, tiled=True)  15.8 us
    dot_general x1, matrix products, per_device(): jnp.einsum('setcf,efd->setcd', activated, expert_down, preferred_element_...  13.5 us
  transfers between devices with their start and end apart: 5, of which 4 were waited for; matrix products, arithmetic and copies ran while one was open for 3% of the time, Pallas kernels for 0%

commit v1 on v0

--- a/solution.py
+++ b/solution.py
@@ -131,7 +131,8 @@
     flat_routes, places = slot_positions(own_routes, 1, expert_count)
     buffer = fill_slots(own_normed, flat_routes, places, 1, expert_count, capacity, exp_local)
     delivered = lax.all_to_all(buffer, "ep", split_axis=0, concat_axis=0, tiled=True)
-    arrived = lax.all_gather(delivered, "tp", axis=2, tiled=True)
+    shards = lax.all_gather(delivered, "tp", axis=0, tiled=False)
+    arrived = jnp.concatenate(shards, axis=2)
     own_flat = flat_routes[0]
     own_places = places[0]
     gates = gate_weights(own_normed, own_routes, router_group, router_expert)

time: 385 us -> 387 us (level)
  transfers between devices with their start and end apart: 5 -> 5, of which waited for: 4 -> 4; matrix products, arithmetic and copies ran while one was open for 3% -> 4% of each run, Pallas kernels for 0% -> 0%
where the time goes in v1:
time: 387 us; the launch traced here: 386 us
  waiting for transfers between devices  236 us (61%)
  blocking collectives  55.6 us (14%)
  matrix products  31.3 us (8%)
  local copies, waits for them, and re-layouts  28.3 us (7%)
  between operations  14.1 us (4%)
  other arithmetic  11.5 us (3%)
  starting transfers between devices  9.19 us (2%)
    unnamed x4, waiting for transfers between devices  140 us
    all_gather x1, waiting for transfers between devices, per_device(): shards = lax.all_gather(delivered, 'tp', axis=0, tiled=False)  57.4 us
    all_to_all x1, blocking collectives, per_device(): lax.all_to_all(buffer, 'ep', split_axis=0, concat_axis=0, tiled=True)  55.6 us
    all_gather x1, waiting for transfers between devices, per_device(): lax.all_gather(attended, 'tp', axis=1, tiled=True)  22.5 us
    all_to_all x1, waiting for transfers between devices, per_device(): lax.all_to_all(summed, 'ep', split_axis=0, concat_axis=0, tiled=True)  15.9 us
    dot_general x1, matrix products, per_device(): jnp.einsum('setcf,efd->setcd', activated, expert_down, preferred_element_...  13.5 us
  transfers between devices with their start and end apart: 5, of which 4 were waited for; matrix products, arithmetic and copies ran while one was open for 4% of the time, Pallas kernels for 0%

profile of v1, /device:TPU:0, one launch (start us, length us, event | category | flops | bytes accessed | tf_op | source)
XLA Modules:
  0.0 385.9 jit_solution(6763377471499878188)
XLA Ops:
  7.2 0.0 copy-start
  7.2 0.0 all-gather.6.cloned.1.call-start
  7.2 0.8 broadcast_multiply_fusion
  8.1 0.1 copy.64
  8.2 0.1 eq.62
  8.3 0.6 reduce-window.6
  8.9 0.2 slice_reduce_fusion
  9.2 0.1 copy.67
  9.3 0.1 broadcast.263
  9.3 0.1 fusion.49
  9.4 0.1 copy.63
  9.5 0.1 mul.115
  9.7 1.2 fusion.32
  10.9 1.3 fusion.34
  12.2 1.6 broadcast_in_dim.34
  13.8 2.3 reshape.391
  16.0 4.4 %scatter_custom_fusion = bf16[512,2048]{1,0:T(8,128)(2,1)} fusion(s32[256]{0:T(256)S(1)} %bitcast.180, bf16[256,2048]{1,0:T(8,128)(2,1)} %reshape.391, bf16[]{:T(256)} %constant.67.clone.1), kind=kCustom, calls=%fused_computation.39 | custom fusion | bytes 2097664 | tf_op jit(solution)/shard_map/scatter | solution.py:53
  20.5 55.6 %all_to_all.10 = bf16[8,2,1,32,2048]{4,3,1,2,0:T(8,128)(2,1)} all-to-all(bf16[8,2,1,32,2048]{4,3,1,2,0:T(8,128)(2,1)} %bitcast.168), channel_id=1, replica_groups=mesh['ep'=8,'tp'=4] {'ep'}, dimensions={0} | all-to-all | bytes 4194304 | tf_op jit(solution)/shard_map/all_to_all | solution.py:133
  76.1 0.0 all-gather.6.cloned.1.call-update
  76.1 0.0 all-reduce.3.cloned.1.call-start
  76.2 57.4 %all-gather.6.cloned.1.call-done = bf16[32,2,1,32,2048]{4,3,2,1,0:T(8,128)(2,1)} async-done(((bf16[8,2,1,32,2048]{4,3,2,1,0:T(8,128)(2,1)}), bf16[32,2,1,32,2048]{4,3,2,1,0:T(8,128)(2,1)}) %all-gather.6.cloned.1.call-update) | async-done | bytes 8388624 | tf_op jit(solution)/shard_map/all_gather | solution.py:134
  133.5 7.7 %fusion.2 = f32[2,8,4,32,256]{4,3,2,1,0:T(8,128)} fusion(bf16[4,8,2,1,32,2048]{5,4,2,1,0,3:T(8,128)(2,1)} %bitcast.184, bf16[2,2048,256]{2,1,0:T(8,128)(2,1)} %param.23), kind=kOutput, calls=%fused_computation.4 | convolution fusion | flops 2147483648 | bytes 12582912 | tf_op jit(solution)/shard_map/setcd,edf->setcf/dot_general | solution.py:139
  141.2 0.0 copy-done
  141.2 13.5 %convert_bitcast_fusion = bf16[8,2,4,32,2048]{4,3,2,0,1:T(8,128)(2,1)} fusion(bf16[2,256,2048]{2,1,0:T(8,128)(2,1)S(1)} %copy-done, f32[2,8,4,32,256]{4,3,2,1,0:T(8,128)} %fusion.2, bf16[2,2048,256]{2,1,0:T(8,128)(2,1)} %param.24, bf16[4,8,2,1,32,2048]{5,4,2,1,0,3:T(8,128)(2,1)} %bitcast.185), kind=kOutput, calls=%fused_computation.6 | convolution fusion | flops 4302307328 | bytes 23068672 | tf_op jit(solution)/shard_map/setcf,efd->setcd/dot_general | solution.py:144
  154.7 0.0 copy-start.2
  154.7 0.0 all-reduce.3.cloned.1.call-update
  154.7 0.9 copy-done.2
  155.6 0.1 copy-done.3
  155.7 3.6 collective-permute-start
  159.3 0.1 add_compare_fusion
  159.4 0.3 broadcast_and_fusion
  159.7 2.8 reshape.401
  162.7 0.0 copy-done.7
  162.7 0.6 dynamic-slice
  163.3 0.0 collective-permute-done
  163.4 0.0 copy-start.6
  163.5 2.1 fusion.7
  165.6 0.0 copy-start.1
  165.6 0.0 copy-done.6
  165.6 0.1 broadcast_maximum_fusion
  165.7 1.1 fusion.6
  166.7 0.8 copy-done.1
  167.5 0.1 exponential_add_fusion
  167.6 140.2 %all-reduce.3.cloned.1.call-done = bf16[8,2,4,32,2048]{4,3,2,0,1:T(8,128)(2,1)} async-done(((bf16[8,2,4,32,2048]{4,3,2,0,1:T(8,128)(2,1)}), bf16[8,2,4,32,2048]{4,3,2,0,1:T(8,128)(2,1)}) %all-reduce.3.cloned.1.call-update) | async-done | bytes 8388624
  307.8 2.4 constant_dynamic-slice_fusion
  310.2 1.4 copy.70
  311.6 5.5 %all-to-all-start.1 = ((bf16[8,2,1,32,2048]{4,3,2,1,0:T(8,128)(2,1)}), bf16[8,2,1,32,2048]{4,3,2,1,0:T(8,128)(2,1)}, u32[]{:S(2)}, u32[]{:S(2)}) async-start(bf16[8,2,1,32,2048]{4,3,2,1,0:T(8,128)(2,1)} %copy.70), calls=%async_computation.1 | async-start | bytes 4194304 | tf_op jit(solution)/shard_map/all_to_all | solution.py:150
  317.1 0.0 all-gather.4.cloned.1.call-start
  317.2 3.4 fusion.29
  320.6 0.0 copy-start.5
  320.6 0.3 copy.61
  320.9 0.9 copy.103
  321.8 0.0 all-gather.4.cloned.1.call-update
  321.8 0.0 copy-done.4
  321.9 0.2 fusion.60
  322.2 0.0 copy-done.5
  322.2 0.3 fusion.59
  322.5 0.1 copy.62
  322.7 22.5 %all-gather.4.cloned.1.call-done = bf16[1024,1024]{0,1:T(8,128)(2,1)} async-done(((bf16[1024,256]{0,1:T(8,128)(2,1)}), bf16[1024,1024]{0,1:T(8,128)(2,1)}) %all-gather.4.cloned.1.call-update) | async-done | bytes 2097168 | tf_op jit(solution)/shard_map/all_gather | solution.py:116
  345.1 4.1 %convolution_convert_fusion = bf16[1024,512]{1,0:T(8,128)(2,1)} fusion(bf16[1024,1024]{0,1:T(8,128)(2,1)} %all-gather.4.cloned.1.call-done, bf16[1024,512]{1,0:T(8,128)(2,1)} %param.17), kind=kOutput, calls=%fused_computation.28 | convolution fusion | flops 1074266112 | bytes 4194304 | tf_op jit(solution)/shard_map/dot_general | solution.py:115
  349.3 15.9 %all-to-all-done.1 = bf16[8,2,1,32,2048]{4,3,2,1,0:T(8,128)(2,1)} async-done(((bf16[8,2,1,32,2048]{4,3,2,1,0:T(8,128)(2,1)}), bf16[8,2,1,32,2048]{4,3,2,1,0:T(8,128)(2,1)}, u32[]{:S(2)}, u32[]{:S(2)}) %all-to-all-start.1) | async-done | bytes 2097184 | tf_op jit(solution)/shard_map/all_to_all | solution.py:150
  365.2 5.2 %gather_fusion = bf16[256,2048]{1,0:T(8,128)(2,1)} fusion(bf16[512,2048]{1,0:T(8,128)(2,1)} %bitcast.39, s32[1024]{0:T(1024)S(1)} %pad_clamp_fusion), kind=kCustom, calls=%fused_computation | custom fusion | bytes 2098176 | tf_op jit(solution)/shard_map/gather | solution.py:152
  370.4 3.4 reshape.378
  373.8 5.6 %multiply_reduce_fusion = bf16[128,2048]{1,0:T(8,128)(2,1)} fusion(f32[128,2,2048]{2,1,0:T(2,128)} %reshape.378, f32[128,2]{1,0:T(8,128)S(1)} %copy.62), kind=kLoop, calls=%fused_computation.26 | loop fusion | flops 786432 | bytes 2622464 | tf_op jit(solution)/shard_map/reduce_sum | solution.py:155
  (35 shorter events, 0.5 us)
Async XLA Ops:
  7.2 134.0 %copy-start = (bf16[2,256,2048]{2,1,0:T(8,128)(2,1)S(1)}, bf16[2,256,2048]{2,1,0:T(8,128)(2,1)}, u32[]{:S(2)}) copy-start(bf16[2,256,2048]{2,1,0:T(8,128)(2,1)} %param.25) | copy-start | bytes 6291460
  7.2 126.4 %all-gather.6.cloned.1.call-start = ((), (), s32[]{:S(2)}) async-start(), calls=%async_computation.3 | async-start | bytes 10485760 | tf_op jit(solution)/shard_map/all_gather | solution.py:134
  76.1 231.7 %all-reduce.3.cloned.1.call-start = ((), (), s32[]{:S(2)}) async-start(), calls=%async_computation.4 | async-start | bytes 16777216
  154.7 0.9 copy-start.2
  154.7 1.0 copy-start.3
  155.6 7.0 %copy-start.7 = (u32[32]{0:T(128)S(1)}, u32[32]{0:T(128)}, u32[]{:S(2)}) copy-start(u32[32]{0:T(128)} %constant.75) | copy-start | bytes 388
  155.7 7.6 %collective-permute-start = (bf16[2,128,64]{1,2,0:T(8,128)(2,1)S(1)}, bf16[2,128,64]{1,2,0:T(8,128)(2,1)S(1)}, u32[]{:S(2)}, u32[]{:S(2)}) collective-permute-start(bf16[2,128,64]{1,2,0:T(8,128)(2,1)S(1)} %pad_maximum_fusion.2), channel_id=1, source_target_pairs={{0,4},{4,8},{8,12},{12,16},{16,20},{20,24},{24,28},{1,5},{5,9},{9,... | collective-permute-start | bytes 98312 | tf_op jit(solution)/shard_map/ppermute | solution.py:15
  163.4 2.2 copy-start.6
  165.6 1.9 copy-start.1
  311.6 53.5 %all-to-all-start.1 = ((bf16[8,2,1,32,2048]{4,3,2,1,0:T(8,128)(2,1)}), bf16[8,2,1,32,2048]{4,3,2,1,0:T(8,128)(2,1)}, u32[]{:S(2)}, u32[]{:S(2)}) async-start(bf16[8,2,1,32,2048]{4,3,2,1,0:T(8,128)(2,1)} %copy.70), calls=%async_computation.1 | async-start | bytes 4194304 | tf_op jit(solution)/shard_map/all_to_all | solution.py:150
  317.1 28.0 %all-gather.4.cloned.1.call-start = ((), (), s32[]{:S(2)}) async-start(), calls=%async_computation.2 | async-start | bytes 2621440 | tf_op jit(solution)/shard_map/all_gather | solution.py:116
  320.6 1.3 copy-start.4
  320.6 1.6 copy-start.5
Sparse Core Ops, SparseCore 0:
  76.2 57.2 all-gather.5
  154.8 152.9 all-reduce.2
  322.0 23.1 all-gather.3
